TPU v7x, 512 devices: a whole 4x4x16 slice. The times are simulated.
512 devices in a mesh: ra: 16 (over y, x), cb: 32 (over z, core).
Axes of the slice: x: 4, y: 4, z: 16, core: 2. Of those that a mesh axis runs over, the one named last changes fastest.
Arguments:
- tokens: bfloat16 [256, 4096], P(None, 'ra'), may hold values from -20 to 20, as said below
- norm_gain: float32 [2, 4096], P(None, 'ra'), may hold values from 0.1 to 1.9
- gate_weight: bfloat16 [2, 4096, 11008], P(None, 'ra', 'cb'), may hold values from -0.09375 to 0.09375
- value_weight: bfloat16 [2, 4096, 11008], P(None, 'ra', 'cb'), may hold values from -0.09375 to 0.09375
- gate_taps: float32 [2, 3, 11008], P(None, None, 'cb'), may hold values from -3.5 to 3.5
- value_taps: float32 [2, 3, 11008], P(None, None, 'cb'), may hold values from -3.5 to 3.5
- down_weight: bfloat16 [2, 11008, 4096], P(None, 'cb', 'ra'), may hold values from -0.0546875 to 0.0546875
Outputs:
- mixed: bfloat16 [256, 4096], P(None, 'ra')
Inputs may be any that keep to these rules, and one draw needn't show every extreme that they name: tokens have features drawn around zero with a scale that varies by blocks of features between about 0.3 and 3.3.
All inputs are finite; a program needn't handle non-finite values.
Results may differ from a plain program's by a relative error of at most 0.0075.
Values may be sent and summed in bfloat16 or wider, within the bound.
A program may use at most 128 MiB of HBM per device.

v0:
```python
import jax
import jax.numpy as jnp
from jax import lax
from jax.sharding import Mesh
from jax.sharding import PartitionSpec as P

D = 4096
RA = ("ra_0", "ra_1")


epsilon = 1e-06


def laid_out(parts, dim):
    shape = list(parts.shape[1:])
    shape[dim] *= parts.shape[0]
    return jnp.moveaxis(parts, 0, dim).reshape(shape)


def copy_for_each(array, axis):
    copies = jnp.broadcast_to(array, (lax.axis_size(axis), *array.shape))
    return lax.all_to_all(copies, axis, split_axis=0, concat_axis=0, tiled=True)


def gathered_copies(array, axis, dim):
    return laid_out(copy_for_each(array, axis), dim)


def shifted(block, axis, distance):
    devices = range(lax.axis_size(axis))
    route = [(i - distance, i) for i in devices if i - distance in devices]
    return lax.ppermute(block, axis, route)


def over_pieces(array, axis):
    return lax.all_gather(array, axis).sum(0)


def split_up(array, dim, peers):
    before, after = (array.shape[:dim], array.shape[dim + 1 :])
    return jnp.moveaxis(array.reshape(*before, peers, -1, *after), dim, 0)


def moved_by_axis(parts, axes, order):
    shape = [lax.axis_size(a) for a in axes]
    parts = parts.reshape(*shape, *parts.shape[1:])
    for k in order:
        parts = lax.all_to_all(parts, axes[k], split_axis=k, concat_axis=k, tiled=True)
    return parts.reshape(-1, *parts.shape[len(axes) :])


def stepwise_exchange(array, axes, order, split_dim, concat_dim):
    parts = split_up(array, split_dim, lax.axis_size(axes))
    return laid_out(moved_by_axis(parts, axes, order), concat_dim)


def conv_after(signal, earlier, kernel_taps):
    length = signal.shape[0]
    width = kernel_taps.shape[0]
    padded = jnp.concatenate([earlier, signal], axis=0)
    result = jnp.zeros(signal.shape, jnp.float32)
    for offset in range(width):
        result = result + kernel_taps[offset] * padded[offset : offset + length]
    return result


def body(tokens, norm_gain, gate_weight, value_weight, gate_taps, value_taps, down_weight):
    stream = lax.all_to_all(tokens, RA, split_axis=0, concat_axis=1, tiled=True)
    gate_whole, value_whole, down_whole = (
        lax.all_gather(gate_weight, RA, axis=1, tiled=True),
        lax.all_gather(value_weight, RA, axis=1, tiled=True),
        lax.all_gather(down_weight, RA, axis=2, tiled=True),
    )
    gain_whole = gathered_copies(norm_gain, RA, 1)
    reach = gate_taps.shape[1] - 1
    for layer_index in range(gate_weight.shape[0]):
        current = stream.astype(jnp.float32)
        inverse_rms = lax.rsqrt(jnp.sum(current * current, axis=1, keepdims=True) / D + epsilon)
        scaled = (current * gain_whole[layer_index]).astype(jnp.bfloat16)
        gate_lin = (
            jnp.dot(scaled, gate_whole[layer_index], preferred_element_type=jnp.float32)
            * inverse_rms
        )
        value_lin = (
            jnp.dot(scaled, value_whole[layer_index], preferred_element_type=jnp.float32)
            * inverse_rms
        )
        tails = jnp.stack(
            [gate_lin[gate_lin.shape[0] - reach :], value_lin[value_lin.shape[0] - reach :]]
        )
        earlier = shifted(tails, RA, 1)
        gate_conv = conv_after(gate_lin, earlier[0], gate_taps[layer_index])
        value_conv = conv_after(value_lin, earlier[1], value_taps[layer_index])
        hidden = (jax.nn.silu(gate_conv) * value_conv).astype(jnp.bfloat16)
        partial_branch = jnp.dot(
            hidden, down_whole[layer_index], preferred_element_type=jnp.float32
        )
        branch = over_pieces(partial_branch, "cb")
        stream = (0.5 * current + branch).astype(jnp.bfloat16)
    return stepwise_exchange(stream, RA, (0, 1), 1, 0)


def solution(mesh):
    finer = Mesh(mesh.devices.reshape(4, 4, mesh.shape["cb"]), ("ra_0", "ra_1", "cb"))
    placed = (
        P(None, RA),
        P(None, RA),
        P(None, RA, "cb"),
        P(None, RA, "cb"),
        P(None, None, "cb"),
        P(None, None, "cb"),
        P(None, "cb", RA),
    )
    return jax.shard_map(body, mesh=finer, in_specs=placed, out_specs=P(None, RA), check_vma=False)
```

profile of v0, /device:TPU:1, one launch (start us, length us, event | category | flops | bytes accessed | tf_op | source)
XLA Modules:
  0.0 461.8 jit_solution(13251371283180898121)
XLA Ops:
  6.5 0.0 copy-start
  6.5 0.0 copy-start.1
  6.5 0.0 all-gather.8.cloned.1.call-start
  6.5 0.7 all-gather.8.cloned.1.call-update
  7.3 0.0 all-gather.10.cloned.1.call-start
  7.3 0.7 all-gather.10.cloned.1.call-update
  8.0 0.0 all-gather.12.cloned.1.call-start
  8.1 0.7 all-gather.12.cloned.1.call-update
  8.7 0.7 broadcast_in_dim.2
  9.4 13.8 %all_to_all.28 = f32[16,2,256]{2,1,0:T(2,128)S(1)} all-to-all(f32[16,2,256]{2,1,0:T(2,128)S(1)} %broadcast_in_dim.2), channel_id=1, replica_groups=mesh['ra_0'=4,'ra_1'=4,'cb'=32] {'ra_0','ra_1'}, dimensions={0} | all-to-all | bytes 65536 | tf_op jit(solution)/shard_map/all_to_all | solution.py:22
  23.3 3.5 all-to-all-start
  26.8 0.0 all-gather.14.cloned.1.call-start
  26.9 6.7 %all-to-all-done = bf16[16,16,256]{2,1,0:T(8,128)(2,1)S(1)} async-done(((bf16[16,16,256]{2,1,0:T(8,128)(2,1)}), bf16[16,16,256]{2,1,0:T(8,128)(2,1)S(1)}, u32[]{:S(2)}, u32[]{:S(2)}) %all-to-all-start) | async-done | bytes 131104 | tf_op jit(solution)/shard_map/all_to_all | solution.py:68
  33.6 0.2 fusion.10
  33.8 59.5 %all-gather.8.cloned.1.call-done = bf16[2,4096,344]{1,2,0:T(8,128)(2,1)} async-done(((bf16[2,256,344]{1,2,0:T(8,128)(2,1)}), bf16[2,4096,344]{1,2,0:T(8,128)(2,1)}) %all-gather.8.cloned.1.call-update) | async-done | bytes 5636112 | tf_op jit(solution)/shard_map/all_gather | solution.py:70
  93.3 2.6 fusion.6
  95.9 78.8 %all-gather.10.cloned.1.call-done = bf16[2,4096,344]{1,2,0:T(8,128)(2,1)} async-done(((bf16[2,256,344]{1,2,0:T(8,128)(2,1)}), bf16[2,4096,344]{1,2,0:T(8,128)(2,1)}) %all-gather.10.cloned.1.call-update) | async-done | bytes 5636112 | tf_op jit(solution)/shard_map/all_gather | solution.py:71
  174.8 2.6 fusion.7
  177.4 2.8 collective-permute-start
  180.2 0.0 copy-done
  180.2 0.0 copy-done.1
  180.3 0.1 slice_reduce_fusion.2
  180.3 0.7 collective-permute-done
  181.0 75.3 %all-gather.12.cloned.1.call-done = bf16[2,344,4096]{2,1,0:T(8,128)(2,1)} async-done(((bf16[2,344,256]{2,1,0:T(8,128)(2,1)}), bf16[2,344,4096]{2,1,0:T(8,128)(2,1)}) %all-gather.12.cloned.1.call-update) | async-done | bytes 5636112 | tf_op jit(solution)/shard_map/all_gather | solution.py:72
  256.2 3.1 fusion.3
  259.4 0.0 all-gather.14.cloned.1.call-update
  259.4 0.0 all-gather.16.cloned.1.call-start
  259.4 80.1 %all-gather.14.cloned.1.call-done = f32[512,4096]{1,0:T(8,128)} async-done(((f32[16,4096]{1,0:T(8,128)}), f32[512,4096]{1,0:T(8,128)}) %all-gather.14.cloned.1.call-update) | async-done | bytes 8388624 | tf_op jit(solution)/shard_map/all_gather | solution.py:36
  339.5 3.8 reduce_sum.41
  343.3 0.1 copy.24
  343.4 0.3 fusion.16
  343.8 2.6 fusion.8
  346.4 2.6 fusion.9
  349.1 3.2 collective-permute-start.1
  352.3 0.8 collective-permute-done.1
  353.1 3.1 fusion
  356.2 0.0 all-gather.16.cloned.1.call-update
  356.2 77.1 %all-gather.16.cloned.1.call-done = f32[512,4096]{1,0:T(8,128)} async-done(((f32[16,4096]{1,0:T(8,128)}), f32[512,4096]{1,0:T(8,128)}) %all-gather.16.cloned.1.call-update) | async-done | bytes 8388624 | tf_op jit(solution)/shard_map/all_gather | solution.py:36
  433.3 3.8 reduce_sum.44
  437.1 0.1 copy.26
  437.3 8.7 %all_to_all.29 = bf16[4,4,16,256]{3,1,2,0:T(4,128)(2,1)S(1)} all-to-all(bf16[4,4,16,256]{3,1,2,0:T(4,128)(2,1)S(1)} %copy.18), channel_id=1, replica_groups=mesh['ra_0'=4,'ra_1'=4,'cb'=32] {'ra_0'}, dimensions={0} | all-to-all | bytes 262144 | tf_op jit(solution)/shard_map/all_to_all | solution.py:48
  446.0 0.1 copy.19
  446.1 8.5 %all_to_all.30 = bf16[4,4,16,256]{3,0,2,1:T(4,128)(2,1)S(1)} all-to-all(bf16[4,4,16,256]{3,0,2,1:T(4,128)(2,1)S(1)} %copy.19), channel_id=1, replica_groups=mesh['ra_0'=4,'ra_1'=4,'cb'=32] {'ra_1'}, dimensions={1} | all-to-all | bytes 262144 | tf_op jit(solution)/shard_map/all_to_all | solution.py:48
  454.6 0.7 copy.20
  (19 shorter events, 0.3 us)
Async XLA Ops:
  6.5 173.7 %copy-start = (f32[2,3,344]{2,0,1:T(2,128)S(1)}, f32[2,3,344]{2,0,1:T(2,128)}, u32[]{:S(2)}) copy-start(f32[2,3,344]{2,0,1:T(2,128)} %param.12) | copy-start | bytes 24772
  6.5 173.7 %copy-start.1 = (f32[2,3,344]{2,0,1:T(2,128)S(1)}, f32[2,3,344]{2,0,1:T(2,128)}, u32[]{:S(2)}) copy-start(f32[2,3,344]{2,0,1:T(2,128)} %param.11) | copy-start | bytes 24772
  6.5 86.7 %all-gather.8.cloned.1.call-start = ((), (), s32[]{:S(2)}) async-start(), calls=%async_computation.4 | async-start | bytes 5988352 | tf_op jit(solution)/shard_map/all_gather | solution.py:70
  7.3 167.5 %all-gather.10.cloned.1.call-start = ((), (), s32[]{:S(2)}) async-start(), calls=%async_computation.5 | async-start | bytes 5988352 | tf_op jit(solution)/shard_map/all_gather | solution.py:71
  8.0 248.2 %all-gather.12.cloned.1.call-start = ((), (), s32[]{:S(2)}) async-start(), calls=%async_computation.6 | async-start | bytes 5988352 | tf_op jit(solution)/shard_map/all_gather | solution.py:72
  23.3 10.3 %all-to-all-start = ((bf16[16,16,256]{2,1,0:T(8,128)(2,1)}), bf16[16,16,256]{2,1,0:T(8,128)(2,1)S(1)}, u32[]{:S(2)}, u32[]{:S(2)}) async-start(bf16[16,16,256]{2,1,0:T(8,128)(2,1)} %bitcast.87), calls=%async_computation | async-start | bytes 262144 | tf_op jit(solution)/shard_map/all_to_all | solution.py:68
  26.8 312.8 %all-gather.14.cloned.1.call-start = ((), (), s32[]{:S(2)}) async-start(), calls=%async_computation.7 | async-start | bytes 8650752 | tf_op jit(solution)/shard_map/all_gather | solution.py:36
  177.4 3.6 collective-permute-start
  259.4 173.9 %all-gather.16.cloned.1.call-start = ((), (), s32[]{:S(2)}) async-start(), calls=%async_computation.8 | async-start | bytes 8650752 | tf_op jit(solution)/shard_map/all_gather | solution.py:36
  349.1 4.0 collective-permute-start.1
Sparse Core Ops, SparseCore 0:
  10.3 82.9 all-gather.7
  96.3 78.4 all-gather.9
  177.7 78.4 all-gather.11
  259.5 79.9 all-gather.13
  356.3 76.9 all-gather.15
where the time goes:
time: 464 us; the launch traced here: 462 us
  waiting for transfers between devices  381 us (82%)
  blocking collectives  31.1 us (7%)
  matrix products  16.7 us (4%)
  between operations  13.4 us (3%)
  starting transfers between devices  9.67 us (2%)
  other arithmetic  8.1 us (2%)
    all_gather x2, waiting for transfers between devices, over_pieces(): return lax.all_gather(array, axis).sum(0)  157 us
    all_gather x1, waiting for transfers between devices, body(): lax.all_gather(value_weight, RA, axis=1, tiled=True)  78.8 us
    all_gather x1, waiting for transfers between devices, body(): lax.all_gather(down_weight, RA, axis=2, tiled=True)  75.3 us
    all_gather x1, waiting for transfers between devices, body(): lax.all_gather(gate_weight, RA, axis=1, tiled=True)  59.5 us
    all_to_all x2, blocking collectives, moved_by_axis(): lax.all_to_all(parts, axes[k], split_axis=k, concat_axis=k, tiled=True)  17.2 us
    all_to_all x1, blocking collectives, copy_for_each(): return lax.all_to_all(copies, axis, split_axis=0, concat_axis=0, tiled=True)  13.8 us
  transfers between devices with their start and end apart: 8, of which 8 were waited for; matrix products, arithmetic and copies ran while one was open for 1% of the time, Pallas kernels for 0%

commit v1 on v0

v1 whole, which is shorter than its diff:
```python
import functools

import jax
import jax.numpy as jnp
from jax import lax
from jax.experimental import pallas as pl
from jax.experimental.pallas import tpu as pltpu
from jax.sharding import PartitionSpec as P

MESH = pl.DeviceIdType.MESH
F32, BF16 = jnp.float32, jnp.bfloat16
EPS = 1e-06
ROWS = 16
LANE = 128
STOP = 99


def round_up(n, m):
    return (n + m - 1) // m * m


def kernel(ny, nx, nz, width, tok, gain, gw, vw, gt, vt, dw, out, gain_v, gw_v, vw_v, gt_v, vt_v, dw_v,
           wcat, dcat, tcat, xs, up_send, halo_send, up_recv, halo_recv, conv_buf, hid_all, branch_own, br_send,
           pair_recv, z_send, z_recv, load_sem, send_sem, recv_sem):
    layers, feats, units = gw_v.shape
    pad = round_up(units, LANE)
    tail = pad - LANE
    nr = ny * nx
    tokens = nr * ROWS
    me = lax.axis_index("ra")
    my = lax.axis_index("cb")
    y, x = me // nx, lax.rem(me, nx)
    z, c = my // 2, lax.rem(my, 2)
    other = 1 - c

    def ra_peer(dy, dx):
        return lax.rem(y + dy, ny) * nx + lax.rem(x + dx, nx)

    loads = []
    pairs = [(tok.at[:, :LANE], xs.at[0, 0]), (tok.at[:, LANE:], xs.at[0, 1]), (gain, gain_v), (gw, gw_v), (vw, vw_v), (gt, gt_v), (vt, vt_v), (dw, dw_v)]
    for i, (a, b) in enumerate(pairs):
        copy = pltpu.make_async_copy(a, b, load_sem.at[i])
        copy.start()
        loads.append(copy)

    barrier = pltpu.get_barrier_semaphore()

    def greet_ra(d, carry):
        pl.semaphore_signal(barrier, inc=1, device_id=(ra_peer(d // nx, lax.rem(d, nx)), my), device_id_type=MESH)
        return carry

    def greet_cb(d, carry):
        pl.semaphore_signal(barrier, inc=1, device_id=(me, lax.rem(z + d, nz) * 2 + c), device_id_type=MESH)
        return carry

    lax.fori_loop(1, nz, greet_cb, 0)
    lax.fori_loop(1, nr, greet_ra, 0)
    pl.semaphore_signal(barrier, inc=1, device_id=(me, z * 2 + other), device_id_type=MESH)

    wcat[...] = jnp.zeros_like(wcat)
    dcat[...] = jnp.zeros_like(dcat)
    tcat[...] = jnp.zeros_like(tcat)
    for copy in loads:
        copy.wait()
    for l in range(layers):
        wcat[l, :, :units] = gw_v[l]
        wcat[l, :, pad:pad + units] = vw_v[l]
        dcat[l, :units, :] = dw_v[l]
        tcat[l, :, :units] = gt_v[l]
        tcat[l, :, pad:pad + units] = vt_v[l]

    ra_order = sorted(range(1, nr), key=lambda d: -(min(d // nx, ny - d // nx) + min(d % nx, nx - d % nx)))
    z_order = sorted(range(1, nz), key=lambda d: -min(d, nz - d))
    sends = []

    def wait_all(ref, sem):
        pltpu.make_async_copy(ref, ref, sem).wait()

    stage = 0
    for l in range(layers):
        if STOP < 6 * l + 1:
            break
        cur = jnp.concatenate([xs[l, 0], xs[l, 1]], axis=1).astype(F32)
        ssq = jnp.sum(cur * cur, axis=1, keepdims=True)
        high = ssq.astype(BF16).astype(F32)
        low = ssq - high
        scaled = (cur * gain_v[l:l + 1, :]).astype(BF16)
        up = jnp.dot(scaled, wcat[l], preferred_element_type=F32)
        lane = lax.broadcasted_iota(jnp.int32, (tokens, LANE), 1) + tail
        spare = jnp.where(lane == units, high, jnp.where(lane == units + 1, low, up[:, tail:pad]))
        up_send[l, :, :tail] = up[:, :tail].astype(BF16)
        up_send[l, :, tail:pad] = spare.astype(BF16)
        up_send[l, :, pad:] = up[:, pad:].astype(BF16)
        for t in range(nr):
            halo_send[l, t] = up_send[l, t * ROWS:(t + 1) * ROWS, :].astype(F32)[ROWS - 2:, :].astype(BF16)
        if l == 0:
            pl.semaphore_wait(barrier, nr + nz - 1)
        for d in ra_order:
            peer = ra_peer(d // nx, d % nx)
            pltpu.make_async_remote_copy(
                src_ref=up_send.at[l, pl.ds(pl.multiple_of(peer * ROWS, ROWS), ROWS)], dst_ref=up_recv.at[l, d - 1],
                send_sem=send_sem.at[l, 0], recv_sem=recv_sem.at[l, 0], device_id=(peer, my), device_id_type=MESH).start()
            before = lax.rem(peer + nr - 1, nr)
            pltpu.make_async_remote_copy(
                src_ref=halo_send.at[l, before], dst_ref=halo_recv.at[l, d - 1],
                send_sem=send_sem.at[l, 1], recv_sem=recv_sem.at[l, 1], device_id=(peer, my), device_id_type=MESH).start()
        sends.append((up_recv.at[l], send_sem.at[l, 0]))
        sends.append((halo_recv.at[l], send_sem.at[l, 1]))
        total = up_send[l, pl.ds(pl.multiple_of(me * ROWS, ROWS), ROWS), :].astype(F32)
        edge = halo_send[l, lax.rem(me + nr - 1, nr)].astype(F32)
        wait_all(up_recv.at[l], recv_sem.at[l, 0])
        wait_all(halo_recv.at[l], recv_sem.at[l, 1])
        if STOP < 6 * l + 2:
            break
        for d in range(nr - 1):
            total = total + up_recv[l, d].astype(F32)
            edge = edge + halo_recv[l, d].astype(F32)

        def normed(block):
            spot = lax.broadcasted_iota(jnp.int32, (block.shape[0], LANE), 1) + tail
            held = jnp.logical_or(spot == units, spot == units + 1)
            meansq = jnp.sum(jnp.where(held, block[:, tail:pad], 0.0), axis=1, keepdims=True) / width
            return block * lax.rsqrt(meansq + EPS)

        conv_buf[8:8 + ROWS, :] = normed(total)
        conv_buf[6:8, :] = jnp.where(me > 0, normed(edge), 0.0)
        conv = tcat[l, 0:1, :] * conv_buf[6:6 + ROWS, :]
        conv = conv + tcat[l, 1:2, :] * conv_buf[7:7 + ROWS, :]
        conv = conv + tcat[l, 2:3, :] * conv_buf[8:8 + ROWS, :]
        gate, value = conv[:, :pad], conv[:, pad:]
        hidden = gate / (1.0 + jnp.exp(-gate)) * value
        column = lax.broadcasted_iota(jnp.int32, (ROWS, pad), 1)
        hid_all[l, me] = jnp.where(column < units, hidden, 0.0).astype(BF16)
        for d in ra_order:
            peer = ra_peer(d // nx, d % nx)
            pltpu.make_async_remote_copy(
                src_ref=hid_all.at[l, me], dst_ref=hid_all.at[l, me],
                send_sem=send_sem.at[l, 2], recv_sem=recv_sem.at[l, 2], device_id=(peer, my), device_id_type=MESH).start()
        others = hid_all.at[l, pl.ds(0, nr - 1)]
        sends.append((others, send_sem.at[l, 2]))
        wait_all(others, recv_sem.at[l, 2])
        if STOP < 6 * l + 3:
            break
        hid = hid_all[l].reshape(tokens, pad)
        part = jnp.dot(hid, dcat[l], preferred_element_type=F32)
        for h in range(2):
            piece = part[:, h * LANE:(h + 1) * LANE]
            branch_own[h] = piece
            br_send[l, h] = piece.astype(BF16)
        pair = pltpu.make_async_remote_copy(
            src_ref=br_send.at[l, other], dst_ref=pair_recv.at[l],
            send_sem=send_sem.at[l, 3], recv_sem=recv_sem.at[l, 3], device_id=(me, z * 2 + other), device_id_type=MESH)
        pair.start()
        sends.append((pair_recv.at[l], send_sem.at[l, 3]))
        pair.wait_recv()
        if STOP < 6 * l + 4:
            break
        z_send[l] = (branch_own[c] + pair_recv[l].astype(F32)).astype(BF16)
        for d in z_order:
            to = lax.rem(z + d, nz)
            pltpu.make_async_remote_copy(
                src_ref=z_send.at[l, pl.ds(pl.multiple_of(to * ROWS, ROWS), ROWS)], dst_ref=z_recv.at[l, d - 1],
                send_sem=send_sem.at[l, 4], recv_sem=recv_sem.at[l, 4], device_id=(me, to * 2 + c), device_id_type=MESH).start()
        sends.append((z_recv.at[l], send_sem.at[l, 4]))
        mine = pl.ds(pl.multiple_of(z * ROWS, ROWS), ROWS)
        branch = z_send[l, mine, :].astype(F32)
        wait_all(z_recv.at[l], recv_sem.at[l, 4])
        if STOP < 6 * l + 5:
            break
        for d in range(nz - 1):
            branch = branch + z_recv[l, d].astype(F32)
        xs[l + 1, c, mine, :] = (0.5 * xs[l, c, mine, :].astype(F32) + branch).astype(BF16)
        for d in z_order:
            to = lax.rem(z + d, nz)
            pltpu.make_async_remote_copy(
                src_ref=xs.at[l + 1, c, mine], dst_ref=xs.at[l + 1, c, mine],
                send_sem=send_sem.at[l, 5], recv_sem=recv_sem.at[l, 5], device_id=(me, to * 2 + c), device_id_type=MESH).start()
        sends.append((z_recv.at[l], send_sem.at[l, 5]))
        wait_all(z_recv.at[l], recv_sem.at[l, 5])
        if STOP < 6 * l + 6:
            break
        swap = pltpu.make_async_remote_copy(
            src_ref=xs.at[l + 1, c], dst_ref=xs.at[l + 1, c],
            send_sem=send_sem.at[l, 6], recv_sem=recv_sem.at[l, 6], device_id=(me, z * 2 + other), device_id_type=MESH)
        swap.start()
        sends.append((pair_recv.at[l], send_sem.at[l, 6]))
        swap.wait_recv()

    if STOP == 0:
        pl.semaphore_wait(barrier, nr + nz - 1)
    stores = []
    for h in range(2):
        store = pltpu.make_async_copy(xs.at[layers if STOP > 90 else 0, h], out.at[:, h * LANE:(h + 1) * LANE], load_sem.at[h])
        store.start()
        stores.append(store)
    for ref, sem in sends:
        wait_all(ref, sem)
    for store in stores:
        store.wait()


def run(ny, nx, nz, width, tokens, norm_gain, gate_weight, value_weight, gate_taps, value_taps, down_weight):
    layers, feats, units = gate_weight.shape
    count = tokens.shape[0]
    pad = round_up(units, LANE)
    nr = ny * nx
    taps = gate_taps.shape[1]
    scratch = [
        pltpu.VMEM((layers, feats), F32),
        pltpu.VMEM((layers, feats, units), BF16),
        pltpu.VMEM((layers, feats, units), BF16),
        pltpu.VMEM((layers, taps, units), F32),
        pltpu.VMEM((layers, taps, units), F32),
        pltpu.VMEM((layers, units, feats), BF16),
        pltpu.VMEM((layers, feats, 2 * pad), BF16),
        pltpu.VMEM((layers, pad, feats), BF16),
        pltpu.VMEM((layers, taps, 2 * pad), F32),
        pltpu.VMEM((layers + 1, 2, count, LANE), BF16),
        pltpu.VMEM((layers, count, 2 * pad), BF16),
        pltpu.VMEM((layers, nr, 2, 2 * pad), BF16),
        pltpu.VMEM((layers, nr - 1, ROWS, 2 * pad), BF16),
        pltpu.VMEM((layers, nr - 1, 2, 2 * pad), BF16),
        pltpu.VMEM((8 + ROWS, 2 * pad), F32),
        pltpu.VMEM((layers, nr, ROWS, pad), BF16),
        pltpu.VMEM((2, count, LANE), F32),
        pltpu.VMEM((layers, 2, count, LANE), BF16),
        pltpu.VMEM((layers, count, LANE), BF16),
        pltpu.VMEM((layers, count, LANE), BF16),
        pltpu.VMEM((layers, nz - 1, ROWS, LANE), BF16),
        pltpu.SemaphoreType.DMA((8,)),
        pltpu.SemaphoreType.DMA((layers, 7)),
        pltpu.SemaphoreType.DMA((layers, 7)),
    ]
    return pl.pallas_call(
        functools.partial(kernel, ny, nx, nz, width),
        out_shape=jax.ShapeDtypeStruct(tokens.shape, tokens.dtype),
        in_specs=[pl.BlockSpec(memory_space=pl.ANY)] * 7,
        out_specs=pl.BlockSpec(memory_space=pl.ANY),
        scratch_shapes=scratch,
        compiler_params=pltpu.CompilerParams(collective_id=0, has_side_effects=True, vmem_limit_bytes=40 * 1024 * 1024),
    )(tokens, norm_gain, gate_weight, value_weight, gate_taps, value_taps, down_weight)


def solution(mesh):
    nr, nz = mesh.shape["ra"], mesh.shape["cb"] // 2
    side = int(round(nr ** 0.5))

    def body(tokens, *rest):
        return run(side, side, nz, tokens.shape[1] * nr, tokens, *rest)

    placed = (P(None, "ra"), P(None, "ra"), P(None, "ra", "cb"), P(None, "ra", "cb"), P(None, None, "cb"), P(None, None, "cb"), P(None, "cb", "ra"))
    return jax.shard_map(body, mesh=mesh, in_specs=placed, out_specs=P(None, "ra"), check_vma=False)
```

time: 464 us -> 80.6 us (0.17)
  waiting for transfers between devices: 381 us -> 0 us
  Pallas kernels: 0 us -> 76.7 us
  blocking collectives: 31.1 us -> 0 us
  matrix products: 16.7 us -> 0 us
  between operations: 13.4 us -> 0.07 us
  starting transfers between devices: 9.67 us -> 0 us
  other arithmetic: 8.1 us -> 0 us
    all_gather x5 -> x0, waiting for transfers between devices: 371 us -> none  [the longest x2 157 us: over_pieces(): return lax.all_gather(array, axis).sum(0)]
    pallas_call x0 -> x1, Pallas kernels: none -> 76.7 us  [run(): pl.pallas_call(functools.partial(kernel, ny, nx, nz, width), out_shape=ja...]
    all_to_all x3 -> x0, blocking collectives: 31.1 us -> none  [the longest x2 17.2 us: moved_by_axis(): lax.all_to_all(parts, axes[k], split_axis=k, concat_axis=k, tiled=True)]
    dot_general x6 -> x0, matrix products: 16.7 us -> none  [the longest x2 6.21 us: body(): jnp.dot(hidden, down_whole[layer_index], preferred_element_type=jnp.float32)]
    reduce_sum x3 -> x0, other arithmetic: 7.84 us -> none  [the longest x2 7.57 us: over_pieces(): return lax.all_gather(array, axis).sum(0)]
    all_to_all x1 -> x0, waiting for transfers between devices: 6.71 us -> none  [body(): stream = lax.all_to_all(tokens, RA, split_axis=0, concat_axis=1, tiled=True)]
    ppermute x2 -> x0, starting transfers between devices: 5.99 us -> none  [shifted(): return lax.ppermute(block, axis, route)]
  transfers between devices with their start and end apart: 8 -> 0, of which waited for: 8 -> 0; matrix products, arithmetic and copies ran while one was open for 1% -> 0% of each run, Pallas kernels for 0% -> 0%
where the time goes in v1:
time: 80.6 us; the launch traced here: 80.4 us
  Pallas kernels  76.7 us (95%)
  local copies, waits for them, and re-layouts  3.61 us (4%)
    pallas_call x1, Pallas kernels, run(): pl.pallas_call(functools.partial(kernel, ny, nx, nz, width), out_shape=ja...  76.7 us
    unnamed x15, local copies, waits for them, and re-layouts  3.61 us

profile of v1, /device:TPU:1, one launch (start us, length us, event | category | flops | bytes accessed | tf_op | source)
XLA Modules:
  0.0 80.4 jit_solution(1499545119423196583)
XLA Ops:
  0.0 0.0 copy-start.4
  0.0 0.7 copy.10.gt
  0.7 0.0 copy-done.4
  0.7 0.0 copy-start.3
  0.7 1.2 %copy.8.gw = bf16[2,256,344]{2,1,0:T(8,128)(2,1)S(1)} copy(bf16[2,256,344]{1,2,0:T(8,128)(2,1)} %param.9) | data formatting | bytes 704512 | tf_op args[2]
  2.0 0.0 copy-done.3
  2.0 0.0 copy-start
  2.0 0.0 copy-start.1
  2.0 0.0 copy-start.2
  2.0 0.2 copy.9.vw
  2.3 0.7 copy-done
  3.0 0.0 copy-done.1
  3.0 0.0 copy-done.2
  3.0 76.7 %shard_map.73 = bf16[256,256]{1,0:T(8,128)(2,1)S(1)} custom-call(bf16[256,256]{1,0:T(8,128)(2,1)S(1)} %copy-done.1, f32[2,256]{1,0:T(2,128)S(1)} %copy-done.2, bf16[2,256,344]{2,1,0:T(8,128)(2,1)S(1)} %copy.8.gw, bf16[2,256,344]{2,1,0:T(8,128)(2,1)S(1)} %copy.9.vw, f32[2,3,344]{2,1,0:T(4,128)S(1)} %copy.10.gt, f32[2,3,344]{2,1,0:T(4,128)S(1)} %copy.11.vt, ...), custom_call_target="tpu_custom_call" | custom-call | tf_op jit(solution)/shard_map/pallas_call | solution.py:234
  79.8 0.7 copy.13
  (1 shorter events, 0.0 us)
Async XLA Ops:
  0.0 0.7 copy-start.4
  0.7 1.3 %copy-start.3 = (bf16[2,256,344]{1,2,0:T(8,128)(2,1)S(1)}, bf16[2,256,344]{1,2,0:T(8,128)(2,1)}, u32[]{:S(2)}) copy-start(bf16[2,256,344]{1,2,0:T(8,128)(2,1)} %param.10) | copy-start | bytes 1056772
  2.0 1.0 %copy-start = (bf16[2,344,256]{2,1,0:T(8,128)(2,1)S(1)}, bf16[2,344,256]{2,1,0:T(8,128)(2,1)}, u32[]{:S(2)}) copy-start(bf16[2,344,256]{2,1,0:T(8,128)(2,1)} %dw.1) | copy-start | bytes 1056772
  2.0 1.0 %copy-start.1 = (bf16[256,256]{1,0:T(8,128)(2,1)S(1)}, bf16[256,256]{1,0:T(8,128)(2,1)}, u32[]{:S(2)}) copy-start(bf16[256,256]{1,0:T(8,128)(2,1)} %tok.1) | copy-start | bytes 393220
  2.0 1.0 %copy-start.2 = (f32[2,256]{1,0:T(2,128)S(1)}, f32[2,256]{1,0:T(2,128)}, u32[]{:S(2)}) copy-start(f32[2,256]{1,0:T(2,128)} %gain.1) | copy-start | bytes 6148
